TPU v7x, 32 devices: a whole 2x2x4 slice. The times are simulated.
32 devices in a mesh: ra: 4 (over z), cb: 2 (over y), dp: 4 (over x, core).
Axes of the slice: x: 2, y: 2, z: 4, core: 2. Of those that a mesh axis runs over, the one named last changes fastest.
Arguments:
- tokens: bfloat16 [1792, 4096], P('dp', 'ra'), may hold values from -70 to 70
- norm_in: bfloat16 [4096], P('ra'), may hold values from 0.099609375 to 1.8984375
- w_up: float32 [4096, 16384], P(None, ('ra', 'cb')), may hold values from -0.09375 to 0.09375
- up_scale: float32 [16384], P(('ra', 'cb')), may hold values from 0.5 to 2
- w_down: float32 [16384, 4096], P('ra', 'cb'), may hold values from -0.0625 to 0.0625
- down_scale: float32 [4096], P('cb'), may hold values from 0.5 to 2
- norm_out: float32 [4096], P('cb'), may hold values from 0.1 to 1.9
Outputs:
- result: bfloat16 [1792, 4096], P('dp', 'cb')
All inputs are finite; a program needn't handle non-finite values.
Results may differ from a plain program's by a relative error of at most 0.024.
Values may be sent and summed in bfloat16 or wider, within the bound.
A program may use at most 128 MiB of HBM per device.

v0:
```python
import jax
import jax.numpy as jnp
from jax import lax
from jax.sharding import PartitionSpec as P

epsilon = 1e-06
resid_weight = 0.25


def per_device(tokens, norm_in, w_up, up_scale, w_down, down_scale, norm_out):
    whole_rows, whole_gain = (
        lax.all_gather(tokens, "ra", axis=1, tiled=True),
        lax.all_gather(norm_in, "ra", axis=0, tiled=True),
    )
    whole_float = whole_rows.astype(jnp.float32)
    model_width = whole_float.shape[1]
    inv_in = lax.rsqrt(jnp.mean(whole_float * whole_float, axis=-1) + epsilon)
    normed = (whole_float * whole_gain.astype(jnp.float32)).astype(jnp.bfloat16)
    pre_act = jnp.dot(normed, w_up.astype(jnp.bfloat16), preferred_element_type=jnp.float32)
    pre_act = pre_act * inv_in[:, None] * up_scale
    hidden = jnp.square(jax.nn.relu(pre_act)).astype(jnp.bfloat16)
    down_bf = w_down.astype(jnp.bfloat16)
    quarter = down_bf.shape[1]
    partial_value = jnp.dot(
        lax.all_gather(hidden, "cb", axis=1, tiled=True),
        down_bf,
        preferred_element_type=jnp.float32,
    )
    col_block = lax.axis_index("cb")
    x_quarter = lax.dynamic_slice_in_dim(whole_float, col_block * quarter, quarter, 1)
    down = lax.psum(partial_value.astype(jnp.bfloat16), "ra").astype(jnp.float32)
    mixed = resid_weight * x_quarter + down * down_scale
    total_sq = lax.psum(jnp.sum(mixed * mixed, axis=-1), "cb")
    inv_out = lax.rsqrt(total_sq / model_width + epsilon)
    return (mixed * inv_out[:, None] * norm_out).astype(jnp.bfloat16)


def solution(mesh):
    placed = (
        P("dp", "ra"),
        P("ra"),
        P(None, ("ra", "cb")),
        P(("ra", "cb")),
        P("ra", "cb"),
        P("cb"),
        P("cb"),
    )
    return jax.shard_map(
        per_device, mesh=mesh, in_specs=placed, out_specs=P("dp", "cb"), check_vma=False
    )
```

profile of v0, /device:TPU:0, one launch (start us, length us, event | category | flops | bytes accessed | tf_op | source)
XLA Modules:
  0.0 266.2 jit_solution(17357724036729051572)
XLA Ops:
  6.5 0.0 copy-start.3
  6.5 0.0 all-gather.3.cloned.1.call-start
  6.5 0.7 all-gather.3.cloned.1.call-update
  7.3 0.0 all-gather.5.cloned.1.call-start
  7.3 13.8 %all_gather.10 = bf16[4096]{0:T(1024)(128)(2,1)S(1)} all-gather(bf16[1024]{0:T(1024)(128)(2,1)} %param.8), channel_id=1, replica_groups=mesh['ra'=4,'cb'=2,'dp'=4] {'ra'}, dimensions={0}, use_global_device_ids=true | all-gather | bytes 10240 | tf_op jit(solution)/shard_map/all_gather | solution.py:13
  21.1 62.7 %all-gather.3.cloned.1.call-done = bf16[448,4096]{1,0:T(8,128)(2,1)} async-done(((bf16[448,1024]{1,0:T(8,128)(2,1)}), bf16[448,4096]{1,0:T(8,128)(2,1)}) %all-gather.3.cloned.1.call-update) | async-done | bytes 3670032 | tf_op jit(solution)/shard_map/all_gather | solution.py:12
  83.7 2.8 %multiply_reduce_fusion = f32[448]{0:T(512)S(1)} fusion(bf16[448,4096]{1,0:T(8,128)(2,1)} %all-gather.3.cloned.1.call-done), kind=kLoop, calls=%fused_computation.4 | loop fusion | flops 5504576 | bytes 3671808 | tf_op jit(solution)/shard_map/reduce_sum | solution.py:17
  86.6 0.0 copy-done.3
  86.6 16.5 %multiply_convert_fusion.3 = bf16[448,2048]{1,0:T(8,128)(2,1)} fusion(f32[4096,2048]{1,0:T(8,128)} %param.9, f32[4096]{0:T(1024)S(1)} %convert_element_type.28, bf16[448,4096]{1,0:T(8,128)(2,1)} %all-gather.3.cloned.1.call-done, f32[2048]{0:T(1024)S(1)} %copy-done.3, f32[448]{0:T(512)S(1)} %add_rsqrt_fusion.1), kind=kOutput, calls=%fused_computation.9 | convolution fusion | flops 7534673920 | bytes 39085824 | tf_op jit(solution)/shard_map/dot_general | solution.py:19
  103.1 0.0 all-gather.5.cloned.1.call-update
  103.2 0.0 all-reduce.2.cloned.1.call-start
  103.2 49.5 %all-gather.5.cloned.1.call-done = bf16[448,4096]{1,0:T(8,128)(2,1)} async-done(((bf16[448,2048]{1,0:T(8,128)(2,1)}), bf16[448,4096]{1,0:T(8,128)(2,1)}) %all-gather.5.cloned.1.call-update) | async-done | bytes 3670032 | tf_op jit(solution)/shard_map/all_gather | solution.py:25
  152.7 16.5 %fusion.8 = bf16[448,2048]{1,0:T(8,128)(2,1)} fusion(bf16[448,4096]{1,0:T(8,128)(2,1)} %all-gather.5.cloned.1.call-done, f32[4096,2048]{1,0:T(8,128)} %param.11), kind=kOutput, calls=%fused_computation.12 | convolution fusion | flops 7525498880 | bytes 39059456 | tf_op jit(solution)/shard_map/dot_general | solution.py:24
  169.2 0.0 all-reduce.2.cloned.1.call-update
  169.2 0.0 copy-start.1
  169.2 5.9 %convert_element_type.27 = f32[448,4096]{1,0:T(8,128)} convert(bf16[448,4096]{1,0:T(8,128)(2,1)} %all-gather.3.cloned.1.call-done) | non-fusion elementwise | flops 1835008 | bytes 11010048 | tf_op jit(solution)/shard_map/convert_element_type | solution.py:15
  175.1 0.0 copy-start.2
  175.1 71.8 %all-reduce.2.cloned.1.call-done = bf16[448,2048]{1,0:T(8,128)(2,1)} async-done(((bf16[448,2048]{1,0:T(8,128)(2,1)}), bf16[448,2048]{1,0:T(8,128)(2,1)}) %all-reduce.2.cloned.1.call-update) | async-done | bytes 1835024 | tf_op jit(solution)/shard_map/psum | solution.py:31
  247.0 0.0 copy-done.1
  247.0 3.5 %multiply_reduce_fusion.1 = f32[448]{0:T(512)S(1)} fusion(bf16[448,2048]{1,0:T(8,128)(2,1)} %all-reduce.2.cloned.1.call-done, f32[448,4096]{1,0:T(8,128)} %convert_element_type.27, s32[]{:T(128)S(6)} %select_n.3, f32[2048]{0:T(1024)S(1)} %copy-done.1), kind=kLoop, calls=%fused_computation.7 | loop fusion | flops 5504576 | bytes 5515012 | tf_op jit(solution)/shard_map/reduce_sum | solution.py:33
  250.5 4.9 %psum.15 = f32[448]{0:T(512)S(1)} all-reduce(f32[448]{0:T(512)S(1)} %multiply_reduce_fusion.1), channel_id=1, replica_groups=mesh['ra'=4,'cb'=2,'dp'=4] {'cb'}, use_global_device_ids=true, to_apply=%region_3.4 | all-reduce | flops 448 | bytes 3584 | tf_op jit(solution)/shard_map/psum | solution.py:33
  255.4 0.0 copy-done.2
  255.4 0.0 copy-done
  255.4 4.2 %multiply_convert_fusion.2 = bf16[448,2048]{1,0:T(8,128)(2,1)} fusion(bf16[448,2048]{1,0:T(8,128)(2,1)S(1)} %copy-done, f32[448,4096]{1,0:T(8,128)} %convert_element_type.27, s32[]{:T(128)S(6)} %select_n.3, f32[2048]{0:T(1024)S(1)} %copy-done.2, f32[448]{0:T(512)S(1)} %add_rsqrt_fusion, f32[2048]{0:T(1024)S(1)} %copy-done.1), kind=kLoop, calls=%fused_computation.6 | loop fusion | flops 6422528 | bytes 7358212 | tf_op jit(solution)/shard_map/convert_element_type | solution.py:35
  (4 shorter events, 0.0 us)
Async XLA Ops:
  6.5 80.1 %copy-start.3 = (f32[2048]{0:T(1024)S(1)}, f32[2048]{0:T(1024)}, u32[]{:S(2)}) copy-start(f32[2048]{0:T(1024)} %param.10) | copy-start | bytes 24580
  6.5 77.2 %all-gather.3.cloned.1.call-start = ((), (), s32[]{:S(2)}) async-start(), calls=%async_computation | async-start | bytes 4587520 | tf_op jit(solution)/shard_map/all_gather | solution.py:12
  7.3 145.4 %all-gather.5.cloned.1.call-start = ((), (), s32[]{:S(2)}) async-start(), calls=%async_computation.1 | async-start | bytes 5505024 | tf_op jit(solution)/shard_map/all_gather | solution.py:25
  103.2 143.8 %all-reduce.2.cloned.1.call-start = ((), (), s32[]{:S(2)}) async-start(), calls=%async_computation.2 | async-start | bytes 3670016 | tf_op jit(solution)/shard_map/psum | solution.py:31
  169.2 77.8 %copy-start.1 = (f32[2048]{0:T(1024)S(1)}, f32[2048]{0:T(1024)}, u32[]{:S(2)}) copy-start(f32[2048]{0:T(1024)} %param.12) | copy-start | bytes 24580
  175.1 80.3 %copy-start.2 = (f32[2048]{0:T(1024)S(1)}, f32[2048]{0:T(1024)}, u32[]{:S(2)}) copy-start(f32[2048]{0:T(1024)} %param.13) | copy-start | bytes 24580
  247.0 8.5 %copy-start = (bf16[448,2048]{1,0:T(8,128)(2,1)S(1)}, bf16[448,2048]{1,0:T(8,128)(2,1)}, u32[]{:S(2)}) copy-start(bf16[448,2048]{1,0:T(8,128)(2,1)} %all-reduce.2.cloned.1.call-done) | copy-start | bytes 5505028
Sparse Core Ops, SparseCore 0:
  8.9 74.8 all-gather.2
  103.3 49.3 all-gather.4
  169.3 77.5 all-reduce.1
where the time goes:
time: 266 us
  waiting for transfers between devices  185 us (70%)
  matrix products  33 us (12%)
  blocking collectives  18.7 us (7%)
  other arithmetic  16.5 us (6%)
  between operations  13.1 us (5%)
    psum x1, waiting for transfers between devices, per_device(): lax.psum(partial_value.astype(jnp.bfloat16), 'ra').astype(jnp.float32)  71.8 us
    all_gather x1, waiting for transfers between devices, per_device(): lax.all_gather(tokens, 'ra', axis=1, tiled=True)  62.7 us
    all_gather x1, waiting for transfers between devices, per_device(): lax.all_gather(hidden, 'cb', axis=1, tiled=True)  49.5 us
    dot_general x1, matrix products, per_device(): jnp.dot(normed, w_up.astype(jnp.bfloat16), preferred_element_type=jnp.flo...  16.5 us
    dot_general x1, matrix products, per_device(): jnp.dot(lax.all_gather(hidden, 'cb', axis=1, tiled=True), down_bf, prefer...  16.5 us
    all_gather x1, blocking collectives, per_device(): lax.all_gather(norm_in, 'ra', axis=0, tiled=True)  13.8 us
    convert_element_type x1, other arithmetic, per_device(): whole_float = whole_rows.astype(jnp.float32)  5.91 us
  transfers between devices with their start and end apart: 3, of which 3 were waited for; matrix products, arithmetic and copies ran while one was open for 2% of the time, Pallas kernels for 0%

commit v1 on v0

--- a/solution.py
+++ b/solution.py
@@ -28,7 +28,9 @@
     )
     col_block = lax.axis_index("cb")
     x_quarter = lax.dynamic_slice_in_dim(whole_float, col_block * quarter, quarter, 1)
-    down = lax.psum(partial_value.astype(jnp.bfloat16), "ra").astype(jnp.float32)
+    down = jnp.sum(lax.all_gather(partial_value.astype(jnp.bfloat16), "ra"), axis=0).astype(
+        jnp.float32
+    )
     mixed = resid_weight * x_quarter + down * down_scale
     total_sq = lax.psum(jnp.sum(mixed * mixed, axis=-1), "cb")
     inv_out = lax.rsqrt(total_sq / model_width + epsilon)

time: 266 us -> 326 us (1.23)
  waiting for transfers between devices: 185 us -> 240 us
  other arithmetic: 16.5 us -> 20.7 us
    all_gather x0 -> x1, waiting for transfers between devices: none -> 127 us  [per_device(): lax.all_gather(partial_value.astype(jnp.bfloat16), 'ra')]
    psum x1 -> x0, waiting for transfers between devices: 71.8 us -> none  [per_device(): lax.psum(partial_value.astype(jnp.bfloat16), 'ra').astype(jnp.float32)]
    reduce_sum x0 -> x1, other arithmetic: none -> 4.88 us  [per_device(): jnp.sum(lax.all_gather(partial_value.astype(jnp.bfloat16), 'ra'), axis=0)]
where the time goes in v1:
time: 326 us; the launch traced here: 325 us
  waiting for transfers between devices  240 us (74%)
  matrix products  33 us (10%)
  other arithmetic  20.7 us (6%)
  blocking collectives  18.7 us (6%)
  between operations  13.1 us (4%)
    all_gather x1, waiting for transfers between devices, per_device(): lax.all_gather(partial_value.astype(jnp.bfloat16), 'ra')  127 us
    all_gather x1, waiting for transfers between devices, per_device(): lax.all_gather(tokens, 'ra', axis=1, tiled=True)  62.7 us
    all_gather x1, waiting for transfers between devices, per_device(): lax.all_gather(hidden, 'cb', axis=1, tiled=True)  49.5 us
    dot_general x1, matrix products, per_device(): jnp.dot(normed, w_up.astype(jnp.bfloat16), preferred_element_type=jnp.flo...  16.5 us
    dot_general x1, matrix products, per_device(): jnp.dot(lax.all_gather(hidden, 'cb', axis=1, tiled=True), down_bf, prefer...  16.5 us
    all_gather x1, blocking collectives, per_device(): lax.all_gather(norm_in, 'ra', axis=0, tiled=True)  13.8 us
  transfers between devices with their start and end apart: 3, of which 3 were waited for; matrix products, arithmetic and copies ran while one was open for 2% of the time, Pallas kernels for 0%

profile of v1, /device:TPU:0, one launch (start us, length us, event | category | flops | bytes accessed | tf_op | source)
XLA Modules:
  0.0 325.2 jit_solution(142749960122872238)
XLA Ops:
  6.5 0.0 copy-start.2
  6.5 0.0 all-gather.5.cloned.1.call-start
  6.5 0.7 all-gather.5.cloned.1.call-update
  7.3 0.0 all-gather.7.cloned.1.call-start
  7.3 13.8 %all_gather.16 = bf16[4096]{0:T(1024)(128)(2,1)S(1)} all-gather(bf16[1024]{0:T(1024)(128)(2,1)} %param.8), channel_id=1, replica_groups=mesh['ra'=4,'cb'=2,'dp'=4] {'ra'}, dimensions={0}, use_global_device_ids=true | all-gather | bytes 10240 | tf_op jit(solution)/shard_map/all_gather | solution.py:13
  21.1 62.7 %all-gather.5.cloned.1.call-done = bf16[448,4096]{1,0:T(8,128)(2,1)} async-done(((bf16[448,1024]{1,0:T(8,128)(2,1)}), bf16[448,4096]{1,0:T(8,128)(2,1)}) %all-gather.5.cloned.1.call-update) | async-done | bytes 3670032 | tf_op jit(solution)/shard_map/all_gather | solution.py:12
  83.7 2.8 multiply_reduce_fusion
  86.6 0.0 copy-done.2
  86.6 16.5 %multiply_convert_fusion.3 = bf16[448,2048]{1,0:T(8,128)(2,1)} fusion(f32[4096,2048]{1,0:T(8,128)} %param.9, f32[4096]{0:T(1024)S(1)} %convert_element_type.30, bf16[448,4096]{1,0:T(8,128)(2,1)} %all-gather.5.cloned.1.call-done, f32[2048]{0:T(1024)S(1)} %copy-done.2, f32[448]{0:T(512)S(1)} %add_rsqrt_fusion.1), kind=kOutput, calls=%fused_computation.9 | convolution fusion | flops 7534673920 | bytes 39085824 | tf_op jit(solution)/shard_map/dot_general | solution.py:19
  103.1 0.0 all-gather.7.cloned.1.call-update
  103.2 0.0 all-gather.9.cloned.1.call-start
  103.2 49.5 %all-gather.7.cloned.1.call-done = bf16[448,4096]{1,0:T(8,128)(2,1)} async-done(((bf16[448,2048]{1,0:T(8,128)(2,1)}), bf16[448,4096]{1,0:T(8,128)(2,1)}) %all-gather.7.cloned.1.call-update) | async-done | bytes 3670032 | tf_op jit(solution)/shard_map/all_gather | solution.py:25
  152.7 16.5 %fusion.8 = bf16[448,2048]{1,0:T(8,128)(2,1)} fusion(bf16[448,4096]{1,0:T(8,128)(2,1)} %all-gather.7.cloned.1.call-done, f32[4096,2048]{1,0:T(8,128)} %param.11), kind=kOutput, calls=%fused_computation.12 | convolution fusion | flops 7525498880 | bytes 39059456 | tf_op jit(solution)/shard_map/dot_general | solution.py:24
  169.2 0.0 all-gather.9.cloned.1.call-update
  169.2 6.0 %convert_element_type.29 = f32[448,4096]{1,0:T(8,128)} convert(bf16[448,4096]{1,0:T(8,128)(2,1)} %all-gather.5.cloned.1.call-done) | non-fusion elementwise | flops 1835008 | bytes 11010048 | tf_op jit(solution)/shard_map/convert_element_type | solution.py:15
  175.2 126.7 %all-gather.9.cloned.1.call-done = bf16[1792,2048]{1,0:T(8,128)(2,1)} async-done(((bf16[448,2048]{1,0:T(8,128)(2,1)}), bf16[1792,2048]{1,0:T(8,128)(2,1)}) %all-gather.9.cloned.1.call-update) | async-done | bytes 7340048 | tf_op jit(solution)/shard_map/all_gather | solution.py:31
  301.8 0.0 copy-start
  301.8 4.9 %reduce_sum.31 = bf16[448,2048]{1,0:T(8,128)(2,1)S(1)} reduce(bf16[4,448,2048]{2,1,0:T(8,128)(2,1)} %bitcast.2, bf16[]{:T(256)} %constant.25.clone.1), dimensions={0}, to_apply=%region_1.2 | reduce | flops 2752512 | bytes 9175042 | tf_op jit(solution)/shard_map/reduce_sum | solution.py:31
  306.7 0.0 copy-done
  306.7 0.0 copy-start.1
  306.7 2.8 multiply_reduce_fusion.1
  309.6 4.9 %psum.7 = f32[448]{0:T(512)S(1)} all-reduce(f32[448]{0:T(512)S(1)} %multiply_reduce_fusion.1), channel_id=1, replica_groups=mesh['ra'=4,'cb'=2,'dp'=4] {'cb'}, use_global_device_ids=true, to_apply=%region_3.4 | all-reduce | flops 448 | bytes 3584 | tf_op jit(solution)/shard_map/psum | solution.py:35
  314.5 0.0 copy-done.1
  314.5 4.2 %multiply_convert_fusion.2 = bf16[448,2048]{1,0:T(8,128)(2,1)} fusion(bf16[448,2048]{1,0:T(8,128)(2,1)S(1)} %reduce_sum.31, f32[448,4096]{1,0:T(8,128)} %convert_element_type.29, s32[]{:T(128)S(6)} %select_n.3, f32[2048]{0:T(1024)S(1)} %copy-done.1, f32[448]{0:T(512)S(1)} %add_rsqrt_fusion, f32[2048]{0:T(1024)S(1)} %copy-done), kind=kLoop, calls=%fused_computation.6 | loop fusion | flops 6422528 | bytes 7358212 | tf_op jit(solution)/shard_map/convert_element_type | solution.py:37
  (3 shorter events, 0.0 us)
Async XLA Ops:
  6.5 80.1 %copy-start.2 = (f32[2048]{0:T(1024)S(1)}, f32[2048]{0:T(1024)}, u32[]{:S(2)}) copy-start(f32[2048]{0:T(1024)} %param.10) | copy-start | bytes 24580
  6.5 77.2 %all-gather.5.cloned.1.call-start = ((), (), s32[]{:S(2)}) async-start(), calls=%async_computation | async-start | bytes 4587520 | tf_op jit(solution)/shard_map/all_gather | solution.py:12
  7.3 145.4 %all-gather.7.cloned.1.call-start = ((), (), s32[]{:S(2)}) async-start(), calls=%async_computation.1 | async-start | bytes 5505024 | tf_op jit(solution)/shard_map/all_gather | solution.py:25
  103.2 198.6 %all-gather.9.cloned.1.call-start = ((), (), s32[]{:S(2)}) async-start(), calls=%async_computation.2 | async-start | bytes 9175040 | tf_op jit(solution)/shard_map/all_gather | solution.py:31
  301.8 4.9 %copy-start = (f32[2048]{0:T(1024)S(1)}, f32[2048]{0:T(1024)}, u32[]{:S(2)}) copy-start(f32[2048]{0:T(1024)} %param.12) | copy-start | bytes 24580
  306.7 7.8 %copy-start.1 = (f32[2048]{0:T(1024)S(1)}, f32[2048]{0:T(1024)}, u32[]{:S(2)}) copy-start(f32[2048]{0:T(1024)} %param.13) | copy-start | bytes 24580
Sparse Core Ops, SparseCore 0:
  8.9 74.8 all-gather.4
  103.3 49.3 all-gather.6
  169.3 132.4 all-gather.8

commit v2 on v0

--- a/solution.py
+++ b/solution.py
@@ -22,7 +22,7 @@
     down_bf = w_down.astype(jnp.bfloat16)
     quarter = down_bf.shape[1]
     partial_value = jnp.dot(
-        lax.all_gather(hidden, "cb", axis=1, tiled=True),
+        jnp.concatenate(lax.all_gather(hidden, "cb"), axis=1),
         down_bf,
         preferred_element_type=jnp.float32,
     )

time: 266 us -> 274 us (1.030)
  local copies, waits for them, and re-layouts: 0.02 us -> 7.9 us
    all_gather x0 -> x1, local copies, waits for them, and re-layouts: none -> 5.81 us  [per_device(): lax.all_gather(hidden, 'cb')]
where the time goes in v2:
time: 274 us
  waiting for transfers between devices  185 us (68%)
  matrix products  32.6 us (12%)
  blocking collectives  18.7 us (7%)
  other arithmetic  16.5 us (6%)
  between operations  13.1 us (5%)
  local copies, waits for them, and re-layouts  7.9 us (3%)
    psum x1, waiting for transfers between devices, per_device(): lax.psum(partial_value.astype(jnp.bfloat16), 'ra').astype(jnp.float32)  71.8 us
    all_gather x1, waiting for transfers between devices, per_device(): lax.all_gather(tokens, 'ra', axis=1, tiled=True)  62.7 us
    all_gather x1, waiting for transfers between devices, per_device(): lax.all_gather(hidden, 'cb')  49.3 us
    dot_general x1, matrix products, per_device(): jnp.dot(normed, w_up.astype(jnp.bfloat16), preferred_element_type=jnp.flo...  16.5 us
    dot_general x1, matrix products, per_device(): jnp.dot(jnp.concatenate(lax.all_gather(hidden, 'cb'), axis=1), down_bf, p...  16 us
    all_gather x1, blocking collectives, per_device(): lax.all_gather(norm_in, 'ra', axis=0, tiled=True)  13.8 us
    convert_element_type x1, other arithmetic, per_device(): whole_float = whole_rows.astype(jnp.float32)  5.91 us
    all_gather x1, local copies, waits for them, and re-layouts, per_device(): lax.all_gather(hidden, 'cb')  5.81 us
  transfers between devices with their start and end apart: 3, of which 3 were waited for; matrix products, arithmetic and copies ran while one was open for 2% of the time, Pallas kernels for 0%

profile of v2, /device:TPU:0, one launch (start us, length us, event | category | flops | bytes accessed | tf_op | source)
XLA Modules:
  0.0 273.6 jit_solution(14719512042375907088)
XLA Ops:
  6.5 0.0 all-gather.4.cloned.1.call-start
  6.5 0.7 all-gather.4.cloned.1.call-update
  7.3 0.0 all-gather.6.cloned.1.call-start
  7.3 13.8 %all_gather.13 = bf16[4096]{0:T(1024)(128)(2,1)S(1)} all-gather(bf16[1024]{0:T(1024)(128)(2,1)} %param.8), channel_id=1, replica_groups=mesh['ra'=4,'cb'=2,'dp'=4] {'ra'}, dimensions={0}, use_global_device_ids=true | all-gather | bytes 10240 | tf_op jit(solution)/shard_map/all_gather | solution.py:13
  21.1 62.7 %all-gather.4.cloned.1.call-done = bf16[448,4096]{1,0:T(8,128)(2,1)} async-done(((bf16[448,1024]{1,0:T(8,128)(2,1)}), bf16[448,4096]{1,0:T(8,128)(2,1)}) %all-gather.4.cloned.1.call-update) | async-done | bytes 3670032 | tf_op jit(solution)/shard_map/all_gather | solution.py:12
  83.7 2.8 %multiply_reduce_fusion = f32[448]{0:T(512)S(1)} fusion(bf16[448,4096]{1,0:T(8,128)(2,1)} %all-gather.4.cloned.1.call-done), kind=kLoop, calls=%fused_computation.4 | loop fusion | flops 5504576 | bytes 3671808 | tf_op jit(solution)/shard_map/reduce_sum | solution.py:17
  86.6 0.0 copy-done.3
  86.6 16.5 %multiply_convert_fusion.3 = bf16[448,2048]{1,0:T(8,128)(2,1)} fusion(f32[4096,2048]{1,0:T(8,128)} %param.9, f32[4096]{0:T(1024)S(1)} %convert_element_type.28, bf16[448,4096]{1,0:T(8,128)(2,1)} %all-gather.4.cloned.1.call-done, f32[2048]{0:T(1024)S(1)} %copy-done.3, f32[448]{0:T(512)S(1)} %add_rsqrt_fusion.1), kind=kOutput, calls=%fused_computation.9 | convolution fusion | flops 7534673920 | bytes 39085824 | tf_op jit(solution)/shard_map/dot_general | solution.py:19
  103.1 0.0 all-gather.6.cloned.1.call-update
  103.2 0.2 all-reduce.2.cloned.1.call-start
  103.4 49.3 %all-gather.6.cloned.1.call-done = bf16[896,2048]{1,0:T(8,128)(2,1)} async-done(((bf16[448,2048]{1,0:T(8,128)(2,1)}), bf16[896,2048]{1,0:T(8,128)(2,1)}) %all-gather.6.cloned.1.call-update) | async-done | bytes 3670032 | tf_op jit(solution)/shard_map/all_gather | solution.py:25
  152.7 5.8 %copy.9 = bf16[2,448,2048]{2,0,1:T(2,128)(2,1)S(1)} copy(bf16[2,448,2048]{2,1,0:T(8,128)(2,1)} %bitcast.6) | data formatting | bytes 7340032 | tf_op jit(solution)/shard_map/all_gather | solution.py:25
  158.5 2.1 copy.10
  160.6 16.0 %fusion.8 = bf16[448,2048]{1,0:T(8,128)(2,1)} fusion(bf16[448,4096]{1,0:T(8,128)(2,1)S(1)} %bitcast.7, f32[4096,2048]{1,0:T(8,128)} %param.11), kind=kOutput, calls=%fused_computation.12 | convolution fusion | flops 7525498880 | bytes 39059456 | tf_op jit(solution)/shard_map/dot_general | solution.py:24
  176.6 0.0 all-reduce.2.cloned.1.call-update
  176.7 0.0 copy-start.1
  176.7 5.9 %convert_element_type.27 = f32[448,4096]{1,0:T(8,128)} convert(bf16[448,4096]{1,0:T(8,128)(2,1)} %all-gather.4.cloned.1.call-done) | non-fusion elementwise | flops 1835008 | bytes 11010048 | tf_op jit(solution)/shard_map/convert_element_type | solution.py:15
  182.6 71.8 %all-reduce.2.cloned.1.call-done = bf16[448,2048]{1,0:T(8,128)(2,1)} async-done(((bf16[448,2048]{1,0:T(8,128)(2,1)}), bf16[448,2048]{1,0:T(8,128)(2,1)}) %all-reduce.2.cloned.1.call-update) | async-done | bytes 1835024 | tf_op jit(solution)/shard_map/psum | solution.py:31
  254.4 0.0 copy-done.1
  254.4 3.5 %multiply_reduce_fusion.1 = f32[448]{0:T(512)S(1)} fusion(bf16[448,2048]{1,0:T(8,128)(2,1)} %all-reduce.2.cloned.1.call-done, f32[448,4096]{1,0:T(8,128)} %convert_element_type.27, s32[]{:T(128)S(6)} %select_n.3, f32[2048]{0:T(1024)S(1)} %copy-done.1), kind=kLoop, calls=%fused_computation.7 | loop fusion | flops 5504576 | bytes 5515012 | tf_op jit(solution)/shard_map/reduce_sum | solution.py:33
  257.9 4.9 %psum.15 = f32[448]{0:T(512)S(1)} all-reduce(f32[448]{0:T(512)S(1)} %multiply_reduce_fusion.1), channel_id=1, replica_groups=mesh['ra'=4,'cb'=2,'dp'=4] {'cb'}, use_global_device_ids=true, to_apply=%region_3.4 | all-reduce | flops 448 | bytes 3584 | tf_op jit(solution)/shard_map/psum | solution.py:33
  262.9 0.0 copy-done.2
  262.9 0.0 copy-done
  262.9 4.2 %multiply_convert_fusion.2 = bf16[448,2048]{1,0:T(8,128)(2,1)} fusion(bf16[448,2048]{1,0:T(8,128)(2,1)S(1)} %copy-done, f32[448,4096]{1,0:T(8,128)} %convert_element_type.27, s32[]{:T(128)S(6)} %select_n.3, f32[2048]{0:T(1024)S(1)} %copy-done.2, f32[448]{0:T(512)S(1)} %add_rsqrt_fusion, f32[2048]{0:T(1024)S(1)} %copy-done.1), kind=kLoop, calls=%fused_computation.6 | loop fusion | flops 6422528 | bytes 7358212 | tf_op jit(solution)/shard_map/convert_element_type | solution.py:35
  (6 shorter events, 0.0 us)
Async XLA Ops:
  6.5 80.1 %copy-start.3 = (f32[2048]{0:T(1024)S(1)}, f32[2048]{0:T(1024)}, u32[]{:S(2)}) copy-start(f32[2048]{0:T(1024)} %param.10) | copy-start | bytes 24580
  6.5 77.2 %all-gather.4.cloned.1.call-start = ((), (), s32[]{:S(2)}) async-start(), calls=%async_computation | async-start | bytes 4587520 | tf_op jit(solution)/shard_map/all_gather | solution.py:12
  7.3 145.4 %all-gather.6.cloned.1.call-start = ((), (), s32[]{:S(2)}) async-start(), calls=%async_computation.2 | async-start | bytes 5505024 | tf_op jit(solution)/shard_map/all_gather | solution.py:25
  103.2 151.3 %all-reduce.2.cloned.1.call-start = ((), (), s32[]{:S(2)}) async-start(), calls=%async_computation.1 | async-start | bytes 3670016 | tf_op jit(solution)/shard_map/psum | solution.py:31
  176.7 77.8 %copy-start.1 = (f32[2048]{0:T(1024)S(1)}, f32[2048]{0:T(1024)}, u32[]{:S(2)}) copy-start(f32[2048]{0:T(1024)} %param.12) | copy-start | bytes 24580
  182.6 80.3 %copy-start.2 = (f32[2048]{0:T(1024)S(1)}, f32[2048]{0:T(1024)}, u32[]{:S(2)}) copy-start(f32[2048]{0:T(1024)} %param.13) | copy-start | bytes 24580
  254.4 8.5 %copy-start = (bf16[448,2048]{1,0:T(8,128)(2,1)S(1)}, bf16[448,2048]{1,0:T(8,128)(2,1)}, u32[]{:S(2)}) copy-start(bf16[448,2048]{1,0:T(8,128)(2,1)} %all-reduce.2.cloned.1.call-done) | copy-start | bytes 5505028
Sparse Core Ops, SparseCore 0:
  8.9 74.8 all-gather.3
  103.3 49.3 all-gather.5
  176.8 77.5 all-reduce.1
